TPU v7x, 32 devices: a whole 2x2x4 slice. The times are simulated.
32 devices in a mesh: grp: 2 (over y), fs: 4 (over z), tp: 4 (over x, core).
Axes of the slice: x: 2, y: 2, z: 4, core: 2. Of those that a mesh axis runs over, the one named last changes fastest.
Arguments:
- stream: bfloat16 [2048, 3072], P('tp', ('grp', 'fs')), parts along dimension 1, may hold values from -6 to 6
- mixer_gain: float32 [2048], replicated, may hold values from 0.1 to 1.9
- glu_value: bfloat16 [2048, 1024], P('fs', 'tp'), may hold values from -0.125 to 0.125
- glu_gate: bfloat16 [2048, 1024], P('fs', 'tp'), may hold values from -0.125 to 0.125
- conv_kernel: bfloat16 [31, 1024], replicated, may hold values from -1 to 1
- channel_gain: float32 [1024], replicated, may hold values from 0.1 to 1.9
- conv_out: bfloat16 [2048, 1024], P('fs', 'tp'), may hold values from -0.1875 to 0.1875
- ffn_gain: float32 [2048], replicated, may hold values from 0.1 to 1.9
- ffn_gate: bfloat16 [2048, 5632], P('fs', 'tp'), may hold values from -0.125 to 0.125
- ffn_up: bfloat16 [2048, 5632], P('fs', 'tp'), may hold values from -0.125 to 0.125
- ffn_down: bfloat16 [2048, 5632], P('fs', 'tp'), may hold values from -0.078125 to 0.078125
Outputs:
- result: bfloat16 [2048, 3072], P('tp', ('grp', 'fs')), parts along dimension 1
There are 2 independent parts, one for each index of `grp`. A program takes and returns all parts, laid end to end along the dimension named above; an argument that names none is the same for every part. Nothing has to cross between parts.
All inputs are finite; a program needn't handle non-finite values.
Results may differ from a plain program's by a relative error of at most 0.018.
Values may be sent and summed in bfloat16 or wider, within the bound.
A program may use at most 64 MiB of HBM per device.

v0:
```python
import jax
import jax.numpy as jnp
from jax import lax
from jax.sharding import PartitionSpec as P


def rms_normalize(wide, gain):
    inverse = lax.rsqrt(jnp.mean(wide * wide, axis=0, keepdims=True) + 1e-06)
    return (wide * inverse * gain[:, None]).astype(jnp.bfloat16)


def contract(weight, acts):
    return lax.dot_general(
        weight, acts, (((0,), (0,)), ((), ())), preferred_element_type=jnp.float32
    )


def on_device(
    stream,
    mixer_gain,
    glu_value,
    glu_gate,
    conv_kernel,
    channel_gain,
    conv_out,
    ffn_gain,
    ffn_gate,
    ffn_up,
    ffn_down,
):
    length = stream.shape[1]
    channels = glu_value.shape[1]
    position = lax.axis_index("tp")
    total_channels = channels * lax.axis_size("tp")
    taps = lax.dynamic_slice_in_dim(conv_kernel, position * channels, channels, 1).astype(
        jnp.float32
    )
    gain_local = lax.dynamic_slice_in_dim(channel_gain, position * channels, channels, 0)
    gathered = lax.all_gather(stream, "tp", axis=0, tiled=True)
    normed = rms_normalize(gathered.astype(jnp.float32), mixer_gain)
    value_w, gate_w, out_w = (
        lax.all_gather(glu_value, "fs", axis=0, tiled=True),
        lax.all_gather(glu_gate, "fs", axis=0, tiled=True),
        lax.all_gather(conv_out, "fs", axis=0, tiled=True),
    )
    value_part = contract(value_w, normed)
    gate_part = contract(gate_w, normed)
    gated = (value_part * jax.nn.sigmoid(gate_part)).astype(jnp.bfloat16).astype(jnp.float32)
    padded = jnp.pad(gated, ((0, 0), (taps.shape[0] - 1, 0)))
    conv_sum = jnp.zeros_like(gated)
    for step in range(taps.shape[0]):
        conv_sum = conv_sum + taps[step][:, None] * padded[:, step : step + length]
    sums, squares = lax.psum(
        (jnp.sum(conv_sum, axis=0), jnp.sum(conv_sum * conv_sum, axis=0)), "tp"
    )
    mean_val = sums / total_channels
    mean_sq = squares / total_channels
    scaled = (
        (conv_sum - mean_val[None, :])
        * lax.rsqrt(mean_sq - mean_val * mean_val + 1e-05)[None, :]
        * gain_local[:, None]
    )
    activated = jax.nn.silu(scaled).astype(jnp.bfloat16)
    mixed_sum = lax.psum_scatter(
        jnp.dot(out_w, activated, preferred_element_type=jnp.float32).astype(jnp.bfloat16),
        "tp",
        scatter_dimension=0,
        tiled=True,
    ).astype(jnp.float32)
    middle_wide = stream.astype(jnp.float32) + mixed_sum
    middle = middle_wide.astype(jnp.bfloat16)
    gathered_two = lax.all_gather(middle, "tp", axis=0, tiled=True)
    normed_two = rms_normalize(gathered_two.astype(jnp.float32), ffn_gain)
    gate_whole, up_whole = (
        lax.all_gather(ffn_gate, "fs", axis=0, tiled=True),
        lax.all_gather(ffn_up, "fs", axis=0, tiled=True),
    )
    gate_val = contract(gate_whole, normed_two)
    up_val = contract(up_whole, normed_two)
    hidden = (jax.nn.silu(gate_val) * up_val).astype(jnp.bfloat16)
    down_whole = lax.all_gather(ffn_down, "fs", axis=0, tiled=True)
    ffn_sum = lax.psum_scatter(
        jnp.dot(down_whole, hidden, preferred_element_type=jnp.float32).astype(jnp.bfloat16),
        "tp",
        scatter_dimension=0,
        tiled=True,
    ).astype(jnp.float32)
    return (middle.astype(jnp.float32) + ffn_sum).astype(jnp.bfloat16)


def solution(mesh):
    in_specs = (
        P("tp", ("grp", "fs")),
        P(),
        P("fs", "tp"),
        P("fs", "tp"),
        P(),
        P(),
        P("fs", "tp"),
        P(),
        P("fs", "tp"),
        P("fs", "tp"),
        P("fs", "tp"),
    )
    out_specs = P("tp", ("grp", "fs"))
    return jax.shard_map(
        on_device, mesh=mesh, in_specs=in_specs, out_specs=out_specs, check_vma=False
    )
```

profile of v0, /device:TPU:0, one launch (start us, length us, event | category | flops | bytes accessed | tf_op | source)
XLA Modules:
  0.0 538.9 jit_solution(6192163965069522078)
XLA Ops:
  9.4 0.7 dynamic-slice_convert_fusion
  10.1 0.8 dynamic_slice.7
  10.9 20.4 %all-gather.9.cloned.1.call-done = bf16[2048,384]{1,0:T(8,128)(2,1)} async-done(((bf16[512,384]{1,0:T(8,128)(2,1)}), bf16[2048,384]{1,0:T(8,128)(2,1)}) %all-gather.9.cloned.1.call-update) | async-done | bytes 1572880 | tf_op jit(solution)/shard_map/all_gather | solution.py:39
  31.3 1.8 fusion
  33.1 27.8 %all-gather.13.cloned.1.call-done = bf16[2048,256]{1,0:T(8,128)(2,1)} async-done(((bf16[512,256]{1,0:T(8,128)(2,1)}), bf16[2048,256]{1,0:T(8,128)(2,1)}) %all-gather.13.cloned.1.call-update) | async-done | bytes 1048592 | tf_op jit(solution)/shard_map/all_gather | solution.py:43
  60.9 2.7 fusion.12
  63.6 26.2 %all-gather.11.cloned.1.call-done = bf16[2048,256]{1,0:T(8,128)(2,1)} async-done(((bf16[512,256]{1,0:T(8,128)(2,1)}), bf16[2048,256]{1,0:T(8,128)(2,1)}) %all-gather.11.cloned.1.call-update) | async-done | bytes 1048592 | tf_op jit(solution)/shard_map/all_gather | solution.py:42
  89.8 2.2 fusion.15
  92.1 1.6 fusion.76
  93.7 6.1 %all-reduce.1 = (f32[384]{0:T(512)S(1)}, f32[384]{0:T(512)S(1)}) all-reduce(f32[384]{0:T(512)S(1)} %get-tuple-element.6, f32[384]{0:T(512)S(1)} %get-tuple-element.5), channel_id=1, replica_groups=mesh['grp'=2,'fs'=4,'tp'=4] {'tp'}, use_global_device_ids=true, to_apply=%region_4.5 | all-reduce | flops 768 | bytes 6144 | tf_op jit(solution)/shard_map/psum | solution.py:53
  99.8 18.9 %all-gather.15.cloned.1.call-done = bf16[2048,256]{1,0:T(8,128)(2,1)} async-done(((bf16[512,256]{1,0:T(8,128)(2,1)}), bf16[2048,256]{1,0:T(8,128)(2,1)}) %all-gather.15.cloned.1.call-update) | async-done | bytes 1048592 | tf_op jit(solution)/shard_map/all_gather | solution.py:44
  118.7 3.1 fusion.8
  122.0 27.2 %reduce-scatter.3.cloned.1.call-done = bf16[512,384]{0,1:T(8,128)(2,1)} async-done(((bf16[2048,384]{0,1:T(8,128)(2,1)}), bf16[512,384]{0,1:T(8,128)(2,1)}) %reduce-scatter.3.cloned.1.call-update) | async-done | bytes 393232 | tf_op jit(solution)/shard_map/reduce_scatter | solution.py:64
  149.3 1.8 add_convert_fusion.1
  153.4 17.5 %all-gather.17.cloned.1.call-done = bf16[2048,384]{0,1:T(8,128)(2,1)} async-done(((bf16[512,384]{0,1:T(8,128)(2,1)}), bf16[2048,384]{0,1:T(8,128)(2,1)}) %all-gather.17.cloned.1.call-update) | async-done | bytes 1572880 | tf_op jit(solution)/shard_map/all_gather | solution.py:72
  170.9 1.8 fusion.3
  172.7 106.5 %all-gather.19.cloned.1.call-done = bf16[2048,1408]{1,0:T(8,128)(2,1)} async-done(((bf16[512,1408]{1,0:T(8,128)(2,1)}), bf16[2048,1408]{1,0:T(8,128)(2,1)}) %all-gather.19.cloned.1.call-update) | async-done | bytes 5767184 | tf_op jit(solution)/shard_map/all_gather | solution.py:75
  279.2 7.1 %convolution_bitcast_fusion.1 = f32[1408,384]{0,1:T(8,128)} fusion(bf16[2048,1408]{1,0:T(8,128)(2,1)} %all-gather.19.cloned.1.call-done, bf16[2048,384]{0,1:T(8,128)(2,1)} %all-gather.17.cloned.1.call-done, f32[2048]{0:T(1024)S(1)} %copy-done.5, f32[384]{0:T(512)S(1)} %add_rsqrt_fusion), kind=kOutput, calls=%fused_computation.12 | convolution fusion | flops 2217738240 | bytes 9512448 | tf_op jit(solution)/shard_map/dot_general | solution.py:13
  286.4 99.4 %all-gather.21.cloned.1.call-done = bf16[2048,1408]{1,0:T(8,128)(2,1)} async-done(((bf16[512,1408]{1,0:T(8,128)(2,1)}), bf16[2048,1408]{1,0:T(8,128)(2,1)}) %all-gather.21.cloned.1.call-update) | async-done | bytes 5767184 | tf_op jit(solution)/shard_map/all_gather | solution.py:76
  385.8 106.6 %all-gather.23.cloned.1.call-done = bf16[2048,1408]{1,0:T(8,128)(2,1)} async-done(((bf16[512,1408]{1,0:T(8,128)(2,1)}), bf16[2048,1408]{1,0:T(8,128)(2,1)}) %all-gather.23.cloned.1.call-update) | async-done | bytes 5767184 | tf_op jit(solution)/shard_map/all_gather | solution.py:81
  492.3 11.3 %fusion.9 = bf16[2048,384]{0,1:T(8,128)(2,1)} fusion(bf16[2048,1408]{1,0:T(8,128)(2,1)} %all-gather.23.cloned.1.call-done, bf16[2048,1408]{1,0:T(8,128)(2,1)} %all-gather.21.cloned.1.call-done, f32[1408,384]{0,1:T(8,128)} %convolution_bitcast_fusion.1, bf16[2048,384]{0,1:T(8,128)(2,1)S(1)} %copy-done.2, f32[2048]{0:T(1024)S(1)} %copy-done.5, ...), kind=kOutput, calls=%fused_computation.17 | convolution fusion | flops 4436361216 | bytes 16852480 | tf_op jit(solution)/shard_map/dot_general | solution.py:83
  503.6 26.4 %reduce-scatter.5.cloned.1.call-done = bf16[512,384]{0,1:T(8,128)(2,1)} async-done(((bf16[2048,384]{0,1:T(8,128)(2,1)}), bf16[512,384]{0,1:T(8,128)(2,1)}) %reduce-scatter.5.cloned.1.call-update) | async-done | bytes 393232 | tf_op jit(solution)/shard_map/reduce_scatter | solution.py:82
  530.1 1.1 add_convert_fusion
  531.2 0.9 copy.13
  (38 shorter events, 5.4 us)
Async XLA Ops:
  6.5 54.3 %copy-start.4 = (f32[2048]{0:T(1024)S(1)}, f32[2048]{0:T(1024)}, u32[]{:S(2)}) copy-start(f32[2048]{0:T(1024)} %param.12) | copy-start | bytes 24580
  6.5 24.7 %all-gather.9.cloned.1.call-start = ((), (), s32[]{:S(2)}) async-start(), calls=%async_computation.2 | async-start | bytes 1966080 | tf_op jit(solution)/shard_map/all_gather | solution.py:39
  7.3 53.6 %all-gather.13.cloned.1.call-start = ((), (), s32[]{:S(2)}) async-start(), calls=%async_computation.4 | async-start | bytes 1310720 | tf_op jit(solution)/shard_map/all_gather | solution.py:43
  8.0 81.8 %all-gather.11.cloned.1.call-start = ((), (), s32[]{:S(2)}) async-start(), calls=%async_computation.3 | async-start | bytes 1310720 | tf_op jit(solution)/shard_map/all_gather | solution.py:42
  8.7 109.9 %all-gather.15.cloned.1.call-start = ((), (), s32[]{:S(2)}) async-start(), calls=%async_computation.5 | async-start | bytes 1310720 | tf_op jit(solution)/shard_map/all_gather | solution.py:44
  9.3 140.0 %reduce-scatter.3.cloned.1.call-start = ((), (), s32[]{:S(2)}) async-start(), calls=%async_computation.6 | async-start | bytes 1966080 | tf_op jit(solution)/shard_map/reduce_scatter | solution.py:64
  33.1 56.7 %copy-start.1 = (bf16[2048,384]{1,0:T(8,128)(2,1)S(1)}, bf16[2048,384]{1,0:T(8,128)(2,1)}, u32[]{:S(2)}) copy-start(bf16[2048,384]{1,0:T(8,128)(2,1)} %all-gather.9.cloned.1.call-done) | copy-start | bytes 4718596
  118.6 3.2 copy-start.3
  121.8 49.2 %all-gather.17.cloned.1.call-start = ((), (), s32[]{:S(2)}) async-start(), calls=%async_computation.7 | async-start | bytes 1966080 | tf_op jit(solution)/shard_map/all_gather | solution.py:72
  151.1 128.1 %all-gather.19.cloned.1.call-start = ((), (), s32[]{:S(2)}) async-start(), calls=%async_computation.8 | async-start | bytes 7208960 | tf_op jit(solution)/shard_map/all_gather | solution.py:75
  151.9 127.3 %copy-start.5 = (f32[2048]{0:T(1024)S(1)}, f32[2048]{0:T(1024)}, u32[]{:S(2)}) copy-start(f32[2048]{0:T(1024)} %param.18) | copy-start | bytes 24580
  151.9 233.9 %all-gather.21.cloned.1.call-start = ((), (), s32[]{:S(2)}) async-start(), calls=%async_computation.9 | async-start | bytes 7208960 | tf_op jit(solution)/shard_map/all_gather | solution.py:76
  152.7 339.7 %all-gather.23.cloned.1.call-start = ((), (), s32[]{:S(2)}) async-start(), calls=%async_computation.10 | async-start | bytes 7208960 | tf_op jit(solution)/shard_map/all_gather | solution.py:81
  153.4 376.7 %reduce-scatter.5.cloned.1.call-start = ((), (), s32[]{:S(2)}) async-start(), calls=%async_computation.11 | async-start | bytes 1966080 | tf_op jit(solution)/shard_map/reduce_scatter | solution.py:82
  172.7 319.6 %copy-start.2 = (bf16[2048,384]{0,1:T(8,128)(2,1)S(1)}, bf16[2048,384]{0,1:T(8,128)(2,1)}, u32[]{:S(2)}) copy-start(bf16[2048,384]{0,1:T(8,128)(2,1)} %all-gather.17.cloned.1.call-done) | copy-start | bytes 4718596
  286.4 243.7 %copy-start = (bf16[512,384]{0,1:T(8,128)(2,1)S(1)}, bf16[512,384]{0,1:T(8,128)(2,1)}, u32[]{:S(2)}) copy-start(bf16[512,384]{0,1:T(8,128)(2,1)} %add_convert_fusion.1) | copy-start | bytes 1179652
Sparse Core Ops, SparseCore 0:
  8.9 22.3 all-gather.8
  32.8 27.9 all-gather.12
  62.4 27.3 all-gather.10
  91.3 27.3 all-gather.14
  121.9 27.3 reduce-scatter.2
  151.3 19.6 all-gather.16
  172.5 106.6 all-gather.18
  280.8 104.9 all-gather.20
  387.4 104.9 all-gather.22
  503.8 26.2 reduce-scatter.4
where the time goes:
time: 539 us
  waiting for transfers between devices  482 us (89%)
  matrix products  26.5 us (5%)
  between operations  13.6 us (3%)
  other arithmetic  8.9 us (2%)
  blocking collectives  6.08 us (1%)
    all_gather x1, waiting for transfers between devices, on_device(): down_whole = lax.all_gather(ffn_down, 'fs', axis=0, tiled=True)  107 us
    all_gather x1, waiting for transfers between devices, on_device(): lax.all_gather(ffn_gate, 'fs', axis=0, tiled=True)  106 us
    all_gather x1, waiting for transfers between devices, on_device(): lax.all_gather(ffn_up, 'fs', axis=0, tiled=True)  99.4 us
    all_gather x1, waiting for transfers between devices, on_device(): lax.all_gather(glu_gate, 'fs', axis=0, tiled=True)  27.8 us
    reduce_scatter x1, waiting for transfers between devices, on_device(): lax.psum_scatter(jnp.dot(out_w, activated, preferred_element_type=jnp.flo...  27.2 us
    reduce_scatter x1, waiting for transfers between devices, on_device(): lax.psum_scatter(jnp.dot(down_whole, hidden, preferred_element_type=jnp.f...  26.4 us
    all_gather x1, waiting for transfers between devices, on_device(): lax.all_gather(glu_value, 'fs', axis=0, tiled=True)  26.2 us
    all_gather x1, waiting for transfers between devices, on_device(): gathered = lax.all_gather(stream, 'tp', axis=0, tiled=True)  20.4 us
  transfers between devices with their start and end apart: 10, of which 10 were waited for; matrix products, arithmetic and copies ran while one was open for 4% of the time, Pallas kernels for 0%

commit v1 on v0

--- a/solution.py
+++ b/solution.py
@@ -78,7 +78,12 @@
     gate_val = contract(gate_whole, normed_two)
     up_val = contract(up_whole, normed_two)
     hidden = (jax.nn.silu(gate_val) * up_val).astype(jnp.bfloat16)
-    down_whole = lax.all_gather(ffn_down, "fs", axis=0, tiled=True)
+    ring = [ffn_down]
+    for hop in range(3):
+        ring.append(lax.ppermute(ring[-1], "fs", [(dev, (dev + 1) % 4) for dev in range(4)]))
+    down_whole = jnp.roll(
+        jnp.concatenate(ring[::-1], axis=0), (lax.axis_index("fs") + 1) * ring[0].shape[0], axis=0
+    )
     ffn_sum = lax.psum_scatter(
         jnp.dot(down_whole, hidden, preferred_element_type=jnp.float32).astype(jnp.bfloat16),
         "tp",

time: 539 us -> 498 us (0.924)
  waiting for transfers between devices: 482 us -> 386 us
  starting transfers between devices: 0.35 us -> 36.6 us
  local copies, waits for them, and re-layouts: 1.93 us -> 17.5 us
    ppermute x0 -> x3, waiting for transfers between devices: none -> 154 us  [on_device(): lax.ppermute(ring[-1], 'fs', [(dev, (dev + 1) % 4) for dev in range(4)])]
    all_gather x1 -> x0, waiting for transfers between devices: 107 us -> none  [on_device(): down_whole = lax.all_gather(ffn_down, 'fs', axis=0, tiled=True)]
    all_gather x1, waiting for transfers between devices: 106 us -> 0.02 us  [on_device(): lax.all_gather(ffn_gate, 'fs', axis=0, tiled=True)]
    ppermute x0 -> x3, starting transfers between devices: none -> 36.3 us  [on_device(): lax.ppermute(ring[-1], 'fs', [(dev, (dev + 1) % 4) for dev in range(4)])]
    all_gather x1, waiting for transfers between devices: 99.4 us -> 81.2 us  [on_device(): lax.all_gather(ffn_up, 'fs', axis=0, tiled=True)]
    all_gather x1, waiting for transfers between devices: 17.5 us -> 0.01 us  [on_device(): gathered_two = lax.all_gather(middle, 'tp', axis=0, tiled=True)]
    unnamed x13 -> x22, local copies, waits for them, and re-layouts: 0.21 us -> 14.4 us
    dot_general x3 -> x4, matrix products: 12.1 us -> 18.2 us  [contract(): lax.dot_general(weight, acts, (((0,), (0,)), ((), ())), preferred_element...]
  transfers between devices with their start and end apart: 10 -> 12, of which waited for: 10 -> 10; matrix products, arithmetic and copies ran while one was open for 4% -> 7% of each run, Pallas kernels for 0% -> 0%
where the time goes in v1:
time: 498 us; the launch traced here: 497 us
  waiting for transfers between devices  386 us (78%)
  starting transfers between devices  36.6 us (7%)
  matrix products  29 us (6%)
  local copies, waits for them, and re-layouts  17.5 us (4%)
  between operations  13.3 us (3%)
  other arithmetic  8.92 us (2%)
  blocking collectives  6.08 us (1%)
    ppermute x3, waiting for transfers between devices, on_device(): lax.ppermute(ring[-1], 'fs', [(dev, (dev + 1) % 4) for dev in range(4)])  154 us
    all_gather x1, waiting for transfers between devices, on_device(): lax.all_gather(ffn_up, 'fs', axis=0, tiled=True)  81.2 us
    ppermute x3, starting transfers between devices, on_device(): lax.ppermute(ring[-1], 'fs', [(dev, (dev + 1) % 4) for dev in range(4)])  36.3 us
    all_gather x1, waiting for transfers between devices, on_device(): lax.all_gather(glu_gate, 'fs', axis=0, tiled=True)  27.7 us
    reduce_scatter x1, waiting for transfers between devices, on_device(): lax.psum_scatter(jnp.dot(out_w, activated, preferred_element_type=jnp.flo...  27.3 us
    reduce_scatter x1, waiting for transfers between devices, on_device(): lax.psum_scatter(jnp.dot(down_whole, hidden, preferred_element_type=jnp.f...  26.5 us
    all_gather x1, waiting for transfers between devices, on_device(): lax.all_gather(glu_value, 'fs', axis=0, tiled=True)  26.2 us
    all_gather x1, waiting for transfers between devices, on_device(): gathered = lax.all_gather(stream, 'tp', axis=0, tiled=True)  20.4 us
  transfers between devices with their start and end apart: 12, of which 10 were waited for; matrix products, arithmetic and copies ran while one was open for 7% of the time, Pallas kernels for 0%

profile of v1, /device:TPU:0, one launch (start us, length us, event | category | flops | bytes accessed | tf_op | source)
XLA Modules:
  0.0 497.1 jit_solution(9108394686141437673)
XLA Ops:
  10.9 20.4 %all-gather.8.cloned.1.call-done = bf16[2048,384]{1,0:T(8,128)(2,1)} async-done(((bf16[512,384]{1,0:T(8,128)(2,1)}), bf16[2048,384]{1,0:T(8,128)(2,1)}) %all-gather.8.cloned.1.call-update) | async-done | bytes 1572880 | tf_op jit(solution)/shard_map/all_gather | solution.py:39
  33.1 27.7 %all-gather.12.cloned.1.call-done = bf16[2048,256]{1,0:T(8,128)(2,1)} async-done(((bf16[512,256]{1,0:T(8,128)(2,1)}), bf16[2048,256]{1,0:T(8,128)(2,1)}) %all-gather.12.cloned.1.call-update) | async-done | bytes 1048592 | tf_op jit(solution)/shard_map/all_gather | solution.py:43
  60.9 2.7 fusion.16
  63.6 26.2 %all-gather.10.cloned.1.call-done = bf16[2048,256]{1,0:T(8,128)(2,1)} async-done(((bf16[512,256]{1,0:T(8,128)(2,1)}), bf16[2048,256]{1,0:T(8,128)(2,1)}) %all-gather.10.cloned.1.call-update) | async-done | bytes 1048592 | tf_op jit(solution)/shard_map/all_gather | solution.py:42
  89.8 2.2 fusion.19
  93.7 6.1 %all-reduce.1 = (f32[384]{0:T(512)S(1)}, f32[384]{0:T(512)S(1)}) all-reduce(f32[384]{0:T(512)S(1)} %get-tuple-element.6, f32[384]{0:T(512)S(1)} %get-tuple-element.5), channel_id=1, replica_groups=mesh['grp'=2,'fs'=4,'tp'=4] {'tp'}, use_global_device_ids=true, to_apply=%region_4.5 | all-reduce | flops 768 | bytes 6144 | tf_op jit(solution)/shard_map/psum | solution.py:53
  99.8 18.9 %all-gather.14.cloned.1.call-done = bf16[2048,256]{1,0:T(8,128)(2,1)} async-done(((bf16[512,256]{1,0:T(8,128)(2,1)}), bf16[2048,256]{1,0:T(8,128)(2,1)}) %all-gather.14.cloned.1.call-update) | async-done | bytes 1048592 | tf_op jit(solution)/shard_map/all_gather | solution.py:44
  118.6 3.0 fusion.13
  122.0 27.3 %reduce-scatter.3.cloned.1.call-done = bf16[512,384]{0,1:T(8,128)(2,1)} async-done(((bf16[2048,384]{0,1:T(8,128)(2,1)}), bf16[512,384]{0,1:T(8,128)(2,1)}) %reduce-scatter.3.cloned.1.call-update) | async-done | bytes 393232 | tf_op jit(solution)/shard_map/reduce_scatter | solution.py:64
  149.2 1.8 add_convert_fusion.1
  154.2 36.8 %collective-permute-done = bf16[512,1408]{1,0:T(8,128)(2,1)S(1)} collective-permute-done((bf16[512,1408]{1,0:T(8,128)(2,1)S(1)}, bf16[512,1408]{1,0:T(8,128)(2,1)S(1)}, u32[]{:S(2)}, u32[]{:S(2)}) %collective-permute-start) | collective-permute-done | bytes 1441824 | tf_op jit(solution)/shard_map/ppermute | solution.py:83
  191.0 3.6 collective-permute-start.1
  194.6 64.4 %collective-permute-done.1 = bf16[512,1408]{1,0:T(8,128)(2,1)} collective-permute-done((bf16[512,1408]{1,0:T(8,128)(2,1)S(1)}, bf16[512,1408]{1,0:T(8,128)(2,1)}, u32[]{:S(2)}, u32[]{:S(2)}) %collective-permute-start.1) | collective-permute-done | bytes 1441824 | tf_op jit(solution)/shard_map/ppermute | solution.py:83
  259.0 31.2 %collective-permute-start.2 = (bf16[512,1408]{1,0:T(8,128)(2,1)}, bf16[512,1408]{1,0:T(8,128)(2,1)}, u32[]{:S(2)}, u32[]{:S(2)}) collective-permute-start(bf16[512,1408]{1,0:T(8,128)(2,1)} %collective-permute-done.1), channel_id=1, source_target_pairs={{0,4},{4,8},{8,12},{12,0},{1,5},{5,9},{9,13},{13,1},{2,6},{6,10},{... | collective-permute-start | bytes 4325384 | tf_op jit(solution)/shard_map/ppermute | solution.py:83
  290.1 52.3 %collective-permute-done.2 = bf16[512,1408]{1,0:T(8,128)(2,1)} collective-permute-done((bf16[512,1408]{1,0:T(8,128)(2,1)}, bf16[512,1408]{1,0:T(8,128)(2,1)}, u32[]{:S(2)}, u32[]{:S(2)}) %collective-permute-start.2) | collective-permute-done | bytes 1441824 | tf_op jit(solution)/shard_map/ppermute | solution.py:83
  342.5 2.6 constant_dynamic-update-slice_fusion.7
  345.1 2.6 constant_dynamic-update-slice_fusion.6
  350.1 2.8 constant_dynamic-update-slice_fusion.3
  352.9 2.6 constant_dynamic-update-slice_fusion.2
  359.9 7.3 %convolution_bitcast_fusion.1 = f32[1408,384]{0,1:T(8,128)} fusion(bf16[2048,1408]{1,0:T(8,128)(2,1)} %all-gather.18.cloned.1.call-done, bf16[2048,384]{0,1:T(8,128)(2,1)} %all-gather.16.cloned.1.call-done, f32[2048]{0:T(1024)S(1)} %copy-done.6, f32[384]{0:T(512)S(1)} %add_rsqrt_fusion), kind=kOutput, calls=%fused_computation.14 | convolution fusion | flops 2217738240 | bytes 9512448 | tf_op jit(solution)/shard_map/dot_general | solution.py:13
  367.1 81.2 %all-gather.20.cloned.1.call-done = bf16[2048,1408]{1,0:T(8,128)(2,1)} async-done(((bf16[512,1408]{1,0:T(8,128)(2,1)}), bf16[2048,1408]{1,0:T(8,128)(2,1)}) %all-gather.20.cloned.1.call-update) | async-done | bytes 5767184 | tf_op jit(solution)/shard_map/all_gather | solution.py:76
  448.3 6.0 %fusion.9 = bf16[1408,384]{0,1:T(8,128)(2,1)S(1)} fusion(bf16[2048,1408]{1,0:T(8,128)(2,1)} %all-gather.20.cloned.1.call-done, f32[1408,384]{0,1:T(8,128)} %convolution_bitcast_fusion.1, bf16[2048,384]{0,1:T(8,128)(2,1)S(1)} %copy-done.2, f32[2048]{0:T(1024)S(1)} %copy-done.6, f32[384]{0:T(512)S(1)} %add_rsqrt_fusion), kind=kOutput, calls=%fused_computation.15 | convolution fusion | flops 2220982272 | bytes 10593792 | tf_op jit(solution)/shard_map/dot_general | solution.py:13
  454.3 7.7 %fusion.10 = bf16[2048,384]{0,1:T(8,128)(2,1)} fusion(bf16[1408,384]{0,1:T(8,128)(2,1)S(1)} %fusion.9, bf16[4096,1408]{1,0:T(8,128)(2,1)} %constant_dynamic-update-slice_fusion, s32[]{:T(128)S(6)} %select_n.19), kind=kOutput, calls=%fused_computation.16 | convolution fusion | flops 2215378944 | bytes 8421380 | tf_op jit(solution)/shard_map/dot_general | solution.py:88
  462.0 26.5 %reduce-scatter.5.cloned.1.call-done = bf16[512,384]{0,1:T(8,128)(2,1)} async-done(((bf16[2048,384]{0,1:T(8,128)(2,1)}), bf16[512,384]{0,1:T(8,128)(2,1)}) %reduce-scatter.5.cloned.1.call-update) | async-done | bytes 393232 | tf_op jit(solution)/shard_map/reduce_scatter | solution.py:87
  (52 shorter events, 19.9 us)
Async XLA Ops:
  6.5 24.7 %all-gather.8.cloned.1.call-start = ((), (), s32[]{:S(2)}) async-start(), calls=%async_computation.2 | async-start | bytes 1966080 | tf_op jit(solution)/shard_map/all_gather | solution.py:39
  7.3 53.6 %all-gather.12.cloned.1.call-start = ((), (), s32[]{:S(2)}) async-start(), calls=%async_computation.4 | async-start | bytes 1310720 | tf_op jit(solution)/shard_map/all_gather | solution.py:43
  8.0 81.8 %all-gather.10.cloned.1.call-start = ((), (), s32[]{:S(2)}) async-start(), calls=%async_computation.3 | async-start | bytes 1310720 | tf_op jit(solution)/shard_map/all_gather | solution.py:42
  8.7 109.9 %all-gather.14.cloned.1.call-start = ((), (), s32[]{:S(2)}) async-start(), calls=%async_computation.5 | async-start | bytes 1310720 | tf_op jit(solution)/shard_map/all_gather | solution.py:44
  9.3 139.9 %reduce-scatter.3.cloned.1.call-start = ((), (), s32[]{:S(2)}) async-start(), calls=%async_computation.6 | async-start | bytes 1966080 | tf_op jit(solution)/shard_map/reduce_scatter | solution.py:64
  33.1 56.7 %copy-start.3 = (bf16[2048,384]{1,0:T(8,128)(2,1)S(1)}, bf16[2048,384]{1,0:T(8,128)(2,1)}, u32[]{:S(2)}) copy-start(bf16[2048,384]{1,0:T(8,128)(2,1)} %all-gather.8.cloned.1.call-done) | copy-start | bytes 4718596
  33.1 56.7 %copy-start.5 = (f32[2048]{0:T(1024)S(1)}, f32[2048]{0:T(1024)}, u32[]{:S(2)}) copy-start(f32[2048]{0:T(1024)} %param.12) | copy-start | bytes 24580
  92.1 29.7 %copy-start.4 = (bf16[512,384]{1,0:T(8,128)(2,1)S(1)}, bf16[512,384]{1,0:T(8,128)(2,1)}, u32[]{:S(2)}) copy-start(bf16[512,384]{1,0:T(8,128)(2,1)} %param.11) | copy-start | bytes 1179652
  121.7 31.0 %copy-start = (bf16[512,1408]{1,0:T(8,128)(2,1)S(1)}, bf16[512,1408]{1,0:T(8,128)(2,1)}, u32[]{:S(2)}) copy-start(bf16[512,1408]{1,0:T(8,128)(2,1)} %param.21) | copy-start | bytes 4325380
  121.7 236.3 %all-gather.16.cloned.1.call-start = ((), (), s32[]{:S(2)}) async-start(), calls=%async_computation.7 | async-start | bytes 1966080 | tf_op jit(solution)/shard_map/all_gather | solution.py:72
  151.1 208.7 %all-gather.18.cloned.1.call-start = ((), (), s32[]{:S(2)}) async-start(), calls=%async_computation.8 | async-start | bytes 7208960 | tf_op jit(solution)/shard_map/all_gather | solution.py:75
  151.9 296.4 %all-gather.20.cloned.1.call-start = ((), (), s32[]{:S(2)}) async-start(), calls=%async_computation.9 | async-start | bytes 7208960 | tf_op jit(solution)/shard_map/all_gather | solution.py:76
  152.6 335.9 %reduce-scatter.5.cloned.1.call-start = ((), (), s32[]{:S(2)}) async-start(), calls=%async_computation.10 | async-start | bytes 1966080 | tf_op jit(solution)/shard_map/reduce_scatter | solution.py:87
  152.7 38.3 %collective-permute-start = (bf16[512,1408]{1,0:T(8,128)(2,1)S(1)}, bf16[512,1408]{1,0:T(8,128)(2,1)S(1)}, u32[]{:S(2)}, u32[]{:S(2)}) collective-permute-start(bf16[512,1408]{1,0:T(8,128)(2,1)S(1)} %copy-done), channel_id=1, source_target_pairs={{0,4},{4,8},{8,12},{12,0},{1,5},{5,9},{9,13},{13,1},{2,6},{6,10},{... | collective-permute-start | bytes 4325384 | tf_op jit(solution)/shard_map/ppermute | solution.py:83
  191.0 68.0 %collective-permute-start.1 = (bf16[512,1408]{1,0:T(8,128)(2,1)S(1)}, bf16[512,1408]{1,0:T(8,128)(2,1)}, u32[]{:S(2)}, u32[]{:S(2)}) collective-permute-start(bf16[512,1408]{1,0:T(8,128)(2,1)S(1)} %collective-permute-done), channel_id=1, source_target_pairs={{0,4},{4,8},{8,12},{12,0},{1,5},{5,9},{9,13},{13,1},{2,6},{6,10},{... | collective-permute-start | bytes 4325384 | tf_op jit(solution)/shard_map/ppermute | solution.py:83
  259.0 83.5 %collective-permute-start.2 = (bf16[512,1408]{1,0:T(8,128)(2,1)}, bf16[512,1408]{1,0:T(8,128)(2,1)}, u32[]{:S(2)}, u32[]{:S(2)}) collective-permute-start(bf16[512,1408]{1,0:T(8,128)(2,1)} %collective-permute-done.1), channel_id=1, source_target_pairs={{0,4},{4,8},{8,12},{12,0},{1,5},{5,9},{9,13},{13,1},{2,6},{6,10},{... | collective-permute-start | bytes 4325384 | tf_op jit(solution)/shard_map/ppermute | solution.py:83
  355.5 4.4 copy-start.6
  359.8 88.5 %copy-start.2 = (bf16[2048,384]{0,1:T(8,128)(2,1)S(1)}, bf16[2048,384]{0,1:T(8,128)(2,1)}, u32[]{:S(2)}) copy-start(bf16[2048,384]{0,1:T(8,128)(2,1)} %all-gather.16.cloned.1.call-done) | copy-start | bytes 4718596
  454.2 34.3 %copy-start.1 = (bf16[512,384]{0,1:T(8,128)(2,1)S(1)}, bf16[512,384]{0,1:T(8,128)(2,1)}, u32[]{:S(2)}) copy-start(bf16[512,384]{0,1:T(8,128)(2,1)} %add_convert_fusion.1) | copy-start | bytes 1179652
Sparse Core Ops, SparseCore 0:
  8.9 22.3 all-gather.7
  32.8 27.9 all-gather.11
  62.4 27.3 all-gather.9
  91.3 27.3 all-gather.13
  121.8 27.3 reduce-scatter.2
  151.2 19.6 all-gather.15
  172.5 170.2 all-gather.17
  344.3 103.9 all-gather.19
  462.2 26.3 reduce-scatter.4
